TPU v7x, 32 devices: a whole 2x2x4 slice. The times are simulated.
32 devices in a mesh: rep: 1, fs: 8 (over z, y), tp: 4 (over x, core).
Axes of the slice: x: 2, y: 2, z: 4, core: 2. Of those that a mesh axis runs over, the one named last changes fastest.
Arguments:
- tokens: bfloat16 [4096, 2048], P(('rep', 'fs')), may hold values from -6 to 6
- gate_outer: bfloat16 [2048, 1024], P('fs', 'tp'), may hold values from -0.125 to 0.125
- gate_inner: bfloat16 [2048, 1024], P('fs', 'tp'), may hold values from -0.125 to 0.125
- conv_input: bfloat16 [2048, 1024], P('fs', 'tp'), may hold values from -0.125 to 0.125
- mixer_output: bfloat16 [2048, 1024], P('fs', 'tp'), may hold values from -0.1875 to 0.1875
- conv_taps: float32 [3, 1024], P(None, 'tp'), may hold values from -3 to 3
- mixer_gain: float32 [2048], replicated, may hold values from 0.1 to 1.9
- mixer_shift: float32 [2048], replicated, may hold values from -3 to 3
- up_weight: bfloat16 [2048, 8192], P('fs', 'tp'), may hold values from -0.125 to 0.125
- down_weight: bfloat16 [2048, 8192], P('fs', 'tp'), may hold values from -0.0625 to 0.0625
- channel_gain: float32 [2048], replicated, may hold values from 0.1 to 1.9
- channel_shift: float32 [2048], replicated, may hold values from -3 to 3
Outputs:
- mixed: bfloat16 [4096, 2048], P(('rep', 'fs'))
All inputs are finite; a program needn't handle non-finite values.
Results may differ from a plain program's by a relative error of at most 0.014.
Values may be sent and summed in bfloat16 or wider, within the bound.
A program may use at most 64 MiB of HBM per device.

v0:
```python
import jax
import jax.numpy as jnp
from jax import lax
from jax.sharding import PartitionSpec as P

residual_scale = 8.0**0.25
norm_epsilon = 1e-05


def layer_norm(values, gain, shift):
    row_mean = jnp.mean(values, -1, keepdims=True)
    centered = values - row_mean
    variance = jnp.mean(centered * centered, -1, keepdims=True)
    return centered * lax.rsqrt(variance + norm_epsilon) * gain + shift


def rounded_partial(left, right_t):
    product = lax.dot_general(
        left, right_t, (((1,), (1,)), ((), ())), preferred_element_type=jnp.float32
    )
    return lax.optimization_barrier(product.astype(jnp.bfloat16)).astype(jnp.float32)


def gated_conv(outer_gate, inner_gate, conv_values, conv_taps):
    seq_len = conv_values.shape[0]
    tap_count = conv_taps.shape[0]
    product = inner_gate * conv_values
    padded = jnp.pad(product, ((tap_count - 1, 0), (0, 0)))
    result = jnp.zeros_like(product)
    for tap_index in range(tap_count):
        result = result + conv_taps[tap_index] * padded[tap_index : tap_index + seq_len]
    return (outer_gate * result).astype(jnp.bfloat16)


def local(
    tokens,
    gate_outer,
    gate_inner,
    conv_input,
    mixer_output,
    conv_taps,
    mixer_gain,
    mixer_shift,
    up_weight,
    down_weight,
    channel_gain,
    channel_shift,
):
    seq_len = tokens.shape[0]
    own_rows = seq_len // lax.axis_size("tp")
    own_start = lax.axis_index("tp") * own_rows
    columns = tokens
    outer_gate = jnp.dot(
        columns,
        lax.all_gather(gate_outer, "fs", axis=0, tiled=True),
        preferred_element_type=jnp.float32,
    )
    inner_gate = jnp.dot(
        columns,
        lax.all_gather(gate_inner, "fs", axis=0, tiled=True),
        preferred_element_type=jnp.float32,
    )
    conv_values = jnp.dot(
        columns,
        lax.all_gather(conv_input, "fs", axis=0, tiled=True),
        preferred_element_type=jnp.float32,
    )
    output_weight = lax.all_gather(mixer_output, "fs", axis=0, tiled=True)
    conv_out = gated_conv(outer_gate, inner_gate, conv_values, conv_taps)
    mixer_sum = lax.psum(
        rounded_partial(conv_out, output_weight).astype(jnp.bfloat16), "tp"
    ).astype(jnp.float32)
    first_rows = layer_norm(
        residual_scale * tokens.astype(jnp.float32) + mixer_sum, mixer_gain, mixer_shift
    ).astype(jnp.bfloat16)
    first_own = lax.dynamic_slice_in_dim(first_rows, own_start, own_rows, 0)
    columns = first_rows
    up_product = jnp.dot(
        columns,
        lax.all_gather(up_weight, "fs", axis=0, tiled=True),
        preferred_element_type=jnp.float32,
    )
    down_full = lax.all_gather(down_weight, "fs", axis=0, tiled=True)
    hidden = jnp.square(jax.nn.relu(up_product)).astype(jnp.bfloat16)
    channel_sum = lax.psum_scatter(
        rounded_partial(hidden, down_full).astype(jnp.bfloat16),
        "tp",
        scatter_dimension=0,
        tiled=True,
    ).astype(jnp.float32)
    output_own = layer_norm(
        residual_scale * first_own.astype(jnp.float32) + channel_sum, channel_gain, channel_shift
    ).astype(jnp.bfloat16)
    return lax.all_gather(output_own, "tp", axis=0, tiled=True)


def solution(mesh):
    in_specs = (
        P(("rep", "fs"), None),
        P("fs", "tp"),
        P("fs", "tp"),
        P("fs", "tp"),
        P("fs", "tp"),
        P(None, "tp"),
        P(),
        P(),
        P("fs", "tp"),
        P("fs", "tp"),
        P(),
        P(),
    )
    out_specs = P(("rep", "fs"), None)
    return jax.shard_map(local, mesh=mesh, in_specs=in_specs, out_specs=out_specs, check_vma=False)
```

profile of v0, /device:TPU:0, one launch (start us, length us, event | category | flops | bytes accessed | tf_op | source)
XLA Modules:
  0.0 565.9 jit_solution(9245024707025191946)
XLA Ops:
  6.5 0.7 all-gather.10.cloned.1.call-update
  7.3 0.7 all-gather.12.cloned.1.call-update
  9.4 0.8 fusion.16
  10.2 42.3 %all-gather.10.cloned.1.call-done = bf16[2048,256]{1,0:T(8,128)(2,1)} async-done(((bf16[256,256]{1,0:T(8,128)(2,1)}), bf16[2048,256]{1,0:T(8,128)(2,1)}) %all-gather.10.cloned.1.call-update) | async-done | bytes 1048592 | tf_op jit(solution)/shard_map/all_gather | solution.py:60
  52.5 2.6 fusion.17
  55.1 38.6 %all-gather.12.cloned.1.call-done = bf16[2048,256]{1,0:T(8,128)(2,1)} async-done(((bf16[256,256]{1,0:T(8,128)(2,1)}), bf16[2048,256]{1,0:T(8,128)(2,1)}) %all-gather.12.cloned.1.call-update) | async-done | bytes 1048592 | tf_op jit(solution)/shard_map/all_gather | solution.py:65
  93.6 1.9 convolution_multiply_fusion
  95.6 39.2 %all-gather.14.cloned.1.call-done = bf16[2048,256]{1,0:T(8,128)(2,1)} async-done(((bf16[256,256]{1,0:T(8,128)(2,1)}), bf16[2048,256]{1,0:T(8,128)(2,1)}) %all-gather.14.cloned.1.call-update) | async-done | bytes 1048592 | tf_op jit(solution)/shard_map/all_gather | solution.py:68
  134.8 41.0 %all-gather.8.cloned.1.call-done = bf16[2048,256]{1,0:T(8,128)(2,1)} async-done(((bf16[256,256]{1,0:T(8,128)(2,1)}), bf16[2048,256]{1,0:T(8,128)(2,1)}) %all-gather.8.cloned.1.call-update) | async-done | bytes 1048592 | tf_op jit(solution)/shard_map/all_gather | solution.py:55
  175.8 5.2 convolution_convert_fusion
  181.6 0.7 all-gather.18.cloned.1.call-update
  182.6 48.7 %all-reduce.3.cloned.1.call-done = bf16[512,2048]{1,0:T(8,128)(2,1)} async-done(((bf16[512,2048]{1,0:T(8,128)(2,1)}), bf16[512,2048]{1,0:T(8,128)(2,1)}) %all-reduce.3.cloned.1.call-update) | async-done | bytes 2097168 | tf_op jit(solution)/shard_map/psum | solution.py:70
  231.2 2.5 fusion
  233.7 1.0 multiply_reduce_fusion
  234.8 2.5 add_convert_fusion
  237.3 120.5 %all-gather.16.cloned.1.call-done = bf16[2048,2048]{1,0:T(8,128)(2,1)} async-done(((bf16[256,2048]{1,0:T(8,128)(2,1)}), bf16[2048,2048]{1,0:T(8,128)(2,1)}) %all-gather.16.cloned.1.call-update) | async-done | bytes 8388624 | tf_op jit(solution)/shard_map/all_gather | solution.py:80
  357.8 124.8 %all-gather.18.cloned.1.call-done = bf16[2048,2048]{1,0:T(8,128)(2,1)} async-done(((bf16[256,2048]{1,0:T(8,128)(2,1)}), bf16[2048,2048]{1,0:T(8,128)(2,1)}) %all-gather.18.cloned.1.call-update) | async-done | bytes 8388624 | tf_op jit(solution)/shard_map/all_gather | solution.py:83
  482.6 16.5 %convolution_convert_fusion.1 = bf16[512,2048]{1,0:T(8,128)(2,1)} fusion(bf16[2048,2048]{1,0:T(8,128)(2,1)} %all-gather.18.cloned.1.call-done, bf16[512,2048]{1,0:T(8,128)(2,1)} %add_convert_fusion, bf16[2048,2048]{1,0:T(8,128)(2,1)} %all-gather.16.cloned.1.call-done), kind=kOutput, calls=%fused_computation.6 | convolution fusion | flops 8594128896 | bytes 20971520 | tf_op jit(solution)/shard_map/dot_general | solution.py:18
  499.2 29.4 %reduce-scatter.2.cloned.1.call-done = bf16[128,2048]{1,0:T(8,128)(2,1)} async-done(((bf16[512,2048]{1,0:T(8,128)(2,1)}), bf16[128,2048]{1,0:T(8,128)(2,1)}) %reduce-scatter.2.cloned.1.call-update) | async-done | bytes 524304 | tf_op jit(solution)/shard_map/reduce_scatter | solution.py:85
  528.6 1.3 fusion.2
  529.9 1.4 multiply_reduce_fusion.1
  531.3 2.2 add_convert_fusion.1
  533.5 22.7 %all-gather.20.cloned.1.call-done = bf16[512,2048]{1,0:T(8,128)(2,1)} async-done(((bf16[128,2048]{1,0:T(8,128)(2,1)}), bf16[512,2048]{1,0:T(8,128)(2,1)}) %all-gather.20.cloned.1.call-update) | async-done | bytes 2097168 | tf_op jit(solution)/shard_map/all_gather | solution.py:94
  556.3 3.2 copy.15
  (33 shorter events, 2.3 us)
Async XLA Ops:
  6.5 87.1 %copy-start = (bf16[512,2048]{1,0:T(8,128)(2,1)S(1)}, bf16[512,2048]{1,0:T(8,128)(2,1)}, u32[]{:S(2)}) copy-start(bf16[512,2048]{1,0:T(8,128)(2,1)} %param.12) | copy-start | bytes 6291460
  6.5 46.0 %all-gather.10.cloned.1.call-start = ((), (), s32[]{:S(2)}) async-start(), calls=%async_computation.2 | async-start | bytes 1179648 | tf_op jit(solution)/shard_map/all_gather | solution.py:60
  7.3 86.4 %all-gather.12.cloned.1.call-start = ((), (), s32[]{:S(2)}) async-start(), calls=%async_computation.3 | async-start | bytes 1179648 | tf_op jit(solution)/shard_map/all_gather | solution.py:65
  8.0 126.8 %all-gather.14.cloned.1.call-start = ((), (), s32[]{:S(2)}) async-start(), calls=%async_computation.4 | async-start | bytes 1179648 | tf_op jit(solution)/shard_map/all_gather | solution.py:68
  8.7 167.1 %all-gather.8.cloned.1.call-start = ((), (), s32[]{:S(2)}) async-start(), calls=%async_computation.1 | async-start | bytes 1179648 | tf_op jit(solution)/shard_map/all_gather | solution.py:55
  9.3 221.9 %all-reduce.3.cloned.1.call-start = ((), (), s32[]{:S(2)}) async-start(), calls=%async_computation.5 | async-start | bytes 4194304 | tf_op jit(solution)/shard_map/psum | solution.py:70
  181.0 176.8 %all-gather.16.cloned.1.call-start = ((), (), s32[]{:S(2)}) async-start(), calls=%async_computation.6 | async-start | bytes 9437184 | tf_op jit(solution)/shard_map/all_gather | solution.py:80
  181.6 301.0 %all-gather.18.cloned.1.call-start = ((), (), s32[]{:S(2)}) async-start(), calls=%async_computation.7 | async-start | bytes 9437184 | tf_op jit(solution)/shard_map/all_gather | solution.py:83
  182.3 52.4 %copy-start.3 = (f32[2048]{0:T(1024)S(1)}, f32[2048]{0:T(1024)}, u32[]{:S(2)}) copy-start(f32[2048]{0:T(1024)} %param.19) | copy-start | bytes 24580
  182.3 52.4 %copy-start.4 = (f32[2048]{0:T(1024)S(1)}, f32[2048]{0:T(1024)}, u32[]{:S(2)}) copy-start(f32[2048]{0:T(1024)} %param.18) | copy-start | bytes 24580
  182.3 346.3 %reduce-scatter.2.cloned.1.call-start = ((), (), s32[]{:S(2)}) async-start(), calls=%async_computation.8 | async-start | bytes 2621440 | tf_op jit(solution)/shard_map/reduce_scatter | solution.py:85
  231.2 2.5 copy-start.1
  237.3 291.4 %copy-start.2 = (bf16[512,2048]{1,0:T(8,128)(2,1)S(1)}, bf16[512,2048]{1,0:T(8,128)(2,1)}, u32[]{:S(2)}) copy-start(bf16[512,2048]{1,0:T(8,128)(2,1)} %add_convert_fusion) | copy-start | bytes 6291460
  499.1 32.2 %copy-start.5 = (f32[2048]{0:T(1024)S(1)}, f32[2048]{0:T(1024)}, u32[]{:S(2)}) copy-start(f32[2048]{0:T(1024)} %param.23) | copy-start | bytes 24580
  499.1 32.2 %copy-start.6 = (f32[2048]{0:T(1024)S(1)}, f32[2048]{0:T(1024)}, u32[]{:S(2)}) copy-start(f32[2048]{0:T(1024)} %param.22) | copy-start | bytes 24580
  499.2 57.1 %all-gather.20.cloned.1.call-start = ((), (), s32[]{:S(2)}) async-start(), calls=%async_computation.9 | async-start | bytes 2621440 | tf_op jit(solution)/shard_map/all_gather | solution.py:94
Sparse Core Ops, SparseCore 0:
  9.5 42.9 all-gather.9
  54.6 38.9 all-gather.11
  95.8 38.9 all-gather.13
  136.8 38.9 all-gather.7
  181.1 50.0 all-reduce.2
  233.2 124.5 all-gather.15
  359.9 122.6 all-gather.17
  499.3 29.3 reduce-scatter.1
  533.6 22.5 all-gather.19
where the time goes:
time: 566 us
  waiting for transfers between devices  511 us (90%)
  matrix products  26.2 us (5%)
  between operations  13.3 us (2%)
  other arithmetic  10.9 us (2%)
    all_gather x1, waiting for transfers between devices, local(): down_full = lax.all_gather(down_weight, 'fs', axis=0, tiled=True)  125 us
    all_gather x1, waiting for transfers between devices, local(): lax.all_gather(up_weight, 'fs', axis=0, tiled=True)  121 us
    psum x1, waiting for transfers between devices, local(): lax.psum(rounded_partial(conv_out, output_weight).astype(jnp.bfloat16), '...  48.7 us
    all_gather x1, waiting for transfers between devices, local(): lax.all_gather(gate_inner, 'fs', axis=0, tiled=True)  42.3 us
    all_gather x1, waiting for transfers between devices, local(): lax.all_gather(gate_outer, 'fs', axis=0, tiled=True)  41 us
    all_gather x1, waiting for transfers between devices, local(): output_weight = lax.all_gather(mixer_output, 'fs', axis=0, tiled=True)  39.2 us
    all_gather x1, waiting for transfers between devices, local(): lax.all_gather(conv_input, 'fs', axis=0, tiled=True)  38.6 us
    reduce_scatter x1, waiting for transfers between devices, local(): lax.psum_scatter(rounded_partial(hidden, down_full).astype(jnp.bfloat16),...  29.4 us
  transfers between devices with their start and end apart: 9, of which 9 were waited for; matrix products, arithmetic and copies ran while one was open for 2% of the time, Pallas kernels for 0%

commit v1 on v0

--- a/solution.py
+++ b/solution.py
@@ -5,6 +5,11 @@
 
 residual_scale = 8.0**0.25
 norm_epsilon = 1e-05
+
+
+def gather_and_add(value, axis):
+    terms = lax.all_gather(value, axis)
+    return jnp.sum(terms, axis=0)
 
 
 def layer_norm(values, gain, shift):
@@ -67,7 +72,7 @@
     )
     output_weight = lax.all_gather(mixer_output, "fs", axis=0, tiled=True)
     conv_out = gated_conv(outer_gate, inner_gate, conv_values, conv_taps)
-    mixer_sum = lax.psum(
+    mixer_sum = gather_and_add(
         rounded_partial(conv_out, output_weight).astype(jnp.bfloat16), "tp"
     ).astype(jnp.float32)
     first_rows = layer_norm(

time: 566 us -> 573 us (1.012)
  other arithmetic: 10.9 us -> 18.1 us
    all_gather x0 -> x1, waiting for transfers between devices: none -> 55.6 us  [gather_and_add(): terms = lax.all_gather(value, axis)]
    psum x1 -> x0, waiting for transfers between devices: 48.7 us -> none  [local(): lax.psum(rounded_partial(conv_out, output_weight).astype(jnp.bfloat16), '...]
    all_gather x1, waiting for transfers between devices: 121 us -> 113 us  [local(): lax.all_gather(up_weight, 'fs', axis=0, tiled=True)]
    reduce_sum x0 -> x1, other arithmetic: none -> 7.2 us  [gather_and_add(): return jnp.sum(terms, axis=0)]
  transfers between devices with their start and end apart: 9 -> 9, of which waited for: 9 -> 9; matrix products, arithmetic and copies ran while one was open for 2% -> 3% of each run, Pallas kernels for 0% -> 0%
where the time goes in v1:
time: 573 us
  waiting for transfers between devices  511 us (89%)
  matrix products  26.2 us (5%)
  other arithmetic  18.1 us (3%)
  between operations  13.3 us (2%)
    all_gather x1, waiting for transfers between devices, local(): down_full = lax.all_gather(down_weight, 'fs', axis=0, tiled=True)  125 us
    all_gather x1, waiting for transfers between devices, local(): lax.all_gather(up_weight, 'fs', axis=0, tiled=True)  113 us
    all_gather x1, waiting for transfers between devices, gather_and_add(): terms = lax.all_gather(value, axis)  55.6 us
    all_gather x1, waiting for transfers between devices, local(): lax.all_gather(gate_inner, 'fs', axis=0, tiled=True)  42.3 us
    all_gather x1, waiting for transfers between devices, local(): output_weight = lax.all_gather(mixer_output, 'fs', axis=0, tiled=True)  41 us
    all_gather x1, waiting for transfers between devices, local(): lax.all_gather(gate_outer, 'fs', axis=0, tiled=True)  39.2 us
    all_gather x1, waiting for transfers between devices, local(): lax.all_gather(conv_input, 'fs', axis=0, tiled=True)  38.6 us
    reduce_scatter x1, waiting for transfers between devices, local(): lax.psum_scatter(rounded_partial(hidden, down_full).astype(jnp.bfloat16),...  29.4 us
  transfers between devices with their start and end apart: 9, of which 9 were waited for; matrix products, arithmetic and copies ran while one was open for 3% of the time, Pallas kernels for 0%

profile of v1, /device:TPU:0, one launch (start us, length us, event | category | flops | bytes accessed | tf_op | source)
XLA Modules:
  0.0 572.8 jit_solution(1696427650436035769)
XLA Ops:
  6.5 0.7 all-gather.12.cloned.1.call-update
  7.3 0.7 all-gather.14.cloned.1.call-update
  9.4 0.8 fusion.16
  10.2 42.3 %all-gather.12.cloned.1.call-done = bf16[2048,256]{1,0:T(8,128)(2,1)} async-done(((bf16[256,256]{1,0:T(8,128)(2,1)}), bf16[2048,256]{1,0:T(8,128)(2,1)}) %all-gather.12.cloned.1.call-update) | async-done | bytes 1048592 | tf_op jit(solution)/shard_map/all_gather | solution.py:65
  52.5 2.6 fusion.17
  55.1 38.6 %all-gather.14.cloned.1.call-done = bf16[2048,256]{1,0:T(8,128)(2,1)} async-done(((bf16[256,256]{1,0:T(8,128)(2,1)}), bf16[2048,256]{1,0:T(8,128)(2,1)}) %all-gather.14.cloned.1.call-update) | async-done | bytes 1048592 | tf_op jit(solution)/shard_map/all_gather | solution.py:70
  93.6 1.9 convolution_multiply_fusion
  95.6 39.2 %all-gather.10.cloned.1.call-done = bf16[2048,256]{1,0:T(8,128)(2,1)} async-done(((bf16[256,256]{1,0:T(8,128)(2,1)}), bf16[2048,256]{1,0:T(8,128)(2,1)}) %all-gather.10.cloned.1.call-update) | async-done | bytes 1048592 | tf_op jit(solution)/shard_map/all_gather | solution.py:60
  134.8 41.0 %all-gather.16.cloned.1.call-done = bf16[2048,256]{1,0:T(8,128)(2,1)} async-done(((bf16[256,256]{1,0:T(8,128)(2,1)}), bf16[2048,256]{1,0:T(8,128)(2,1)}) %all-gather.16.cloned.1.call-update) | async-done | bytes 1048592 | tf_op jit(solution)/shard_map/all_gather | solution.py:73
  175.8 5.2 convolution_convert_fusion
  182.5 55.6 %all-gather.24.cloned.1.call-done = bf16[2048,2048]{1,0:T(8,128)(2,1)} async-done(((bf16[512,2048]{1,0:T(8,128)(2,1)}), bf16[2048,2048]{1,0:T(8,128)(2,1)}) %all-gather.24.cloned.1.call-update) | async-done | bytes 8388624 | tf_op jit(solution)/shard_map/all_gather | solution.py:11
  238.1 7.2 %reduce_sum.48 = bf16[512,2048]{1,0:T(8,128)(2,1)} reduce(bf16[4,512,2048]{2,1,0:T(8,128)(2,1)} %bitcast.14, bf16[]{:T(256)} %constant.11.clone.1), dimensions={0}, to_apply=%region_0.1 | reduce | flops 3145728 | bytes 10485762 | tf_op jit(solution)/shard_map/reduce_sum | solution.py:12
  245.3 2.5 fusion
  247.8 1.0 multiply_reduce_fusion
  248.9 2.5 add_convert_fusion
  251.4 113.2 %all-gather.18.cloned.1.call-done = bf16[2048,2048]{1,0:T(8,128)(2,1)} async-done(((bf16[256,2048]{1,0:T(8,128)(2,1)}), bf16[2048,2048]{1,0:T(8,128)(2,1)}) %all-gather.18.cloned.1.call-update) | async-done | bytes 8388624 | tf_op jit(solution)/shard_map/all_gather | solution.py:85
  364.6 124.8 %all-gather.20.cloned.1.call-done = bf16[2048,2048]{1,0:T(8,128)(2,1)} async-done(((bf16[256,2048]{1,0:T(8,128)(2,1)}), bf16[2048,2048]{1,0:T(8,128)(2,1)}) %all-gather.20.cloned.1.call-update) | async-done | bytes 8388624 | tf_op jit(solution)/shard_map/all_gather | solution.py:88
  489.4 16.5 %convolution_convert_fusion.1 = bf16[512,2048]{1,0:T(8,128)(2,1)} fusion(bf16[2048,2048]{1,0:T(8,128)(2,1)} %all-gather.20.cloned.1.call-done, bf16[512,2048]{1,0:T(8,128)(2,1)} %add_convert_fusion, bf16[2048,2048]{1,0:T(8,128)(2,1)} %all-gather.18.cloned.1.call-done), kind=kOutput, calls=%fused_computation.6 | convolution fusion | flops 8594128896 | bytes 20971520 | tf_op jit(solution)/shard_map/dot_general | solution.py:23
  506.0 29.4 %reduce-scatter.2.cloned.1.call-done = bf16[128,2048]{1,0:T(8,128)(2,1)} async-done(((bf16[512,2048]{1,0:T(8,128)(2,1)}), bf16[128,2048]{1,0:T(8,128)(2,1)}) %reduce-scatter.2.cloned.1.call-update) | async-done | bytes 524304 | tf_op jit(solution)/shard_map/reduce_scatter | solution.py:90
  535.5 1.3 fusion.2
  536.8 1.4 multiply_reduce_fusion.1
  538.2 2.2 add_convert_fusion.1
  540.3 22.7 %all-gather.22.cloned.1.call-done = bf16[512,2048]{1,0:T(8,128)(2,1)} async-done(((bf16[128,2048]{1,0:T(8,128)(2,1)}), bf16[512,2048]{1,0:T(8,128)(2,1)}) %all-gather.22.cloned.1.call-update) | async-done | bytes 2097168 | tf_op jit(solution)/shard_map/all_gather | solution.py:99
  563.1 3.2 copy.14
  (34 shorter events, 3.0 us)
Async XLA Ops:
  6.5 87.1 %copy-start = (bf16[512,2048]{1,0:T(8,128)(2,1)S(1)}, bf16[512,2048]{1,0:T(8,128)(2,1)}, u32[]{:S(2)}) copy-start(bf16[512,2048]{1,0:T(8,128)(2,1)} %param.12) | copy-start | bytes 6291460
  6.5 46.0 %all-gather.12.cloned.1.call-start = ((), (), s32[]{:S(2)}) async-start(), calls=%async_computation.2 | async-start | bytes 1179648 | tf_op jit(solution)/shard_map/all_gather | solution.py:65
  7.3 86.4 %all-gather.14.cloned.1.call-start = ((), (), s32[]{:S(2)}) async-start(), calls=%async_computation.3 | async-start | bytes 1179648 | tf_op jit(solution)/shard_map/all_gather | solution.py:70
  8.0 126.8 %all-gather.10.cloned.1.call-start = ((), (), s32[]{:S(2)}) async-start(), calls=%async_computation.1 | async-start | bytes 1179648 | tf_op jit(solution)/shard_map/all_gather | solution.py:60
  8.7 167.1 %all-gather.16.cloned.1.call-start = ((), (), s32[]{:S(2)}) async-start(), calls=%async_computation.4 | async-start | bytes 1179648 | tf_op jit(solution)/shard_map/all_gather | solution.py:73
  9.3 228.8 %all-gather.24.cloned.1.call-start = ((), (), s32[]{:S(2)}) async-start(), calls=%async_computation.9 | async-start | bytes 10485760 | tf_op jit(solution)/shard_map/all_gather | solution.py:11
  181.0 183.6 %all-gather.18.cloned.1.call-start = ((), (), s32[]{:S(2)}) async-start(), calls=%async_computation.5 | async-start | bytes 9437184 | tf_op jit(solution)/shard_map/all_gather | solution.py:85
  181.6 307.9 %all-gather.20.cloned.1.call-start = ((), (), s32[]{:S(2)}) async-start(), calls=%async_computation.6 | async-start | bytes 9437184 | tf_op jit(solution)/shard_map/all_gather | solution.py:88
  182.3 353.1 %reduce-scatter.2.cloned.1.call-start = ((), (), s32[]{:S(2)}) async-start(), calls=%async_computation.7 | async-start | bytes 2621440 | tf_op jit(solution)/shard_map/reduce_scatter | solution.py:90
  245.3 2.5 copy-start.1
  245.3 3.5 copy-start.3
  245.3 3.6 copy-start.4
  251.4 284.1 %copy-start.2 = (bf16[512,2048]{1,0:T(8,128)(2,1)S(1)}, bf16[512,2048]{1,0:T(8,128)(2,1)}, u32[]{:S(2)}) copy-start(bf16[512,2048]{1,0:T(8,128)(2,1)} %add_convert_fusion) | copy-start | bytes 6291460
  505.9 32.2 %copy-start.5 = (f32[2048]{0:T(1024)S(1)}, f32[2048]{0:T(1024)}, u32[]{:S(2)}) copy-start(f32[2048]{0:T(1024)} %param.23) | copy-start | bytes 24580
  505.9 32.2 %copy-start.6 = (f32[2048]{0:T(1024)S(1)}, f32[2048]{0:T(1024)}, u32[]{:S(2)}) copy-start(f32[2048]{0:T(1024)} %param.22) | copy-start | bytes 24580
  506.0 57.1 %all-gather.22.cloned.1.call-start = ((), (), s32[]{:S(2)}) async-start(), calls=%async_computation.8 | async-start | bytes 2621440 | tf_op jit(solution)/shard_map/all_gather | solution.py:99
Sparse Core Ops, SparseCore 0:
  9.5 42.9 all-gather.11
  54.6 38.9 all-gather.13
  95.8 38.9 all-gather.9
  136.8 38.9 all-gather.15
  181.1 56.9 all-gather.23
  240.1 124.4 all-gather.17
  366.7 122.6 all-gather.19
  506.1 29.3 reduce-scatter.1
  540.5 22.5 all-gather.21
